TPU v7x, 32 devices: a whole 2x2x4 slice. The times are simulated.
32 devices in a mesh: sp: 8 (over z, x), tp: 4 (over y, core).
Axes of the slice: x: 2, y: 2, z: 4, core: 2. Of those that a mesh axis runs over, the one named last changes fastest.
Arguments:
- outer_gate: bfloat16 [2048, 2048], P('sp', 'tp'), may hold values from -6 to 6
- inner_gate: bfloat16 [2048, 2048], P('sp', 'tp'), may hold values from -6 to 6
- conv_input: bfloat16 [2048, 2048], P('sp', 'tp'), may hold values from -6 to 6
- conv_weight: bfloat16 [3, 2048], P(None, 'tp'), may hold values from -3.5 to 3.5
- doc_ids: int32 [2048], P('sp'), may hold values from 0 to 3, as said below
- output_weight: bfloat16 [2048, 4096], P(None, 'tp'), may hold values from -0.125 to 0.125
- residual: bfloat16 [2048, 4096], P('sp', 'tp'), as said below
- norm_gain: bfloat16 [4096], P('tp'), may hold values from 0.099609375 to 1.8984375
- expert_ids: int32 [2048, 2], P('sp'), may hold values from 0 to 7, all different within a row; in each aligned block of 256 rows (0 to 255, 256 to 511, ...) at most 128 rows name the same one
- group_weight: float32 [2048], P('sp'), may hold values from 0.25 to 1
- expert_weight: float32 [2048, 2], P('sp'), may hold values from 0.05 to 1
- gate_weight: bfloat16 [8, 4096, 2048], P('sp', None, 'tp'), may hold values from -0.09375 to 0.09375
- up_weight: bfloat16 [8, 4096, 2048], P('sp', None, 'tp'), may hold values from -0.09375 to 0.09375
- down_weight: bfloat16 [8, 2048, 4096], P('sp', None, 'tp'), may hold values from -0.125 to 0.125
Outputs:
- layer_out: bfloat16 [2048, 4096], P('sp', 'tp')
Inputs may be any that keep to these rules, and one draw needn't show every extreme that they name: `expert_ids`: within the 256 rows of one index of sp no expert is named more than 128 times, a bound that some block reaches; the two experts of a row differ. `doc_ids`: never falling along positions, rising by one at each document's start; every document has 256 to 768 positions, and one exactly 768. `residual`: Columns' scales are of order one to ten.
All inputs are finite; a program needn't handle non-finite values.
Results may differ from a plain program's by a relative error of at most 0.009.
Values may be sent and summed in bfloat16 or wider, within the bound.
A program may use at most 64 MiB of HBM per device.

v0:
```python
import jax
import jax.numpy as jnp
from jax import lax
from jax.sharding import PartitionSpec as P

EPS = 1e-06


def passed_along(value, axis, steps):
    count = lax.axis_size(axis)
    initial, last = (max(0, -steps), min(count, count - steps))
    return lax.ppermute(value, axis, [(source, source + steps) for source in range(initial, last)])


def per_device(
    outer_gate,
    inner_gate,
    conv_input,
    conv_weight,
    doc_ids,
    output_weight,
    residual,
    norm_gain,
    expert_ids,
    group_weight,
    expert_weight,
    gate_weight,
    up_weight,
    down_weight,
):
    row_count = conv_input.shape[0]
    products = inner_gate.astype(jnp.float32) * conv_input.astype(jnp.float32)
    own_docs = doc_ids.astype(jnp.float32)
    tail_rows, tail_docs = passed_along((products[-2:], own_docs[-2:]), "sp", 1)
    ext_products = jnp.concatenate([tail_rows, products], axis=0)
    ext_docs = jnp.concatenate([tail_docs, own_docs], axis=0)
    taps = conv_weight.astype(jnp.float32)
    conv = taps[2] * products
    for shift_by in (1, 2):
        first = 2 - shift_by
        same_doc = (ext_docs[first : first + row_count] == own_docs)[:, None]
        conv = conv + jnp.where(
            same_doc, taps[2 - shift_by] * ext_products[first : first + row_count], 0.0
        )
    branch = (outer_gate.astype(jnp.float32) * conv).astype(jnp.bfloat16)
    cols_local = output_weight.shape[1]
    branch_sum = jnp.dot(
        lax.all_gather(branch, "tp", axis=1, tiled=True),
        output_weight,
        preferred_element_type=jnp.float32,
    )
    resid = (residual.astype(jnp.float32) + branch_sum).astype(jnp.bfloat16)
    resid_wide = resid.astype(jnp.float32)
    total_sq = lax.psum(jnp.sum(resid_wide * resid_wide, axis=1), "tp")
    width = cols_local * lax.axis_size("tp")
    scale = lax.rsqrt(total_sq / width + EPS)[:, None]
    normed = (resid_wide * scale * norm_gain.astype(jnp.float32)).astype(jnp.bfloat16)
    experts = lax.axis_size("sp")
    capacity = 4 * row_count // experts
    flat_experts = expert_ids.reshape(-1)
    onehot = (flat_experts[:, None] == jnp.arange(experts, dtype=jnp.int32)[None, :]).astype(
        jnp.int32
    )
    slot_rank = jnp.sum((jnp.cumsum(onehot, axis=0) - onehot) * onehot, axis=1)
    slot_index = flat_experts * capacity + slot_rank
    token_of = jnp.arange(2 * row_count, dtype=jnp.int32) // 2
    token_table = jnp.full((experts * capacity,), row_count, jnp.int32).at[slot_index].set(token_of)
    gate_local = gate_weight[0]
    up_local = up_weight[0]
    arrived_rows = experts * capacity
    padded = jnp.concatenate([normed, jnp.zeros((1, cols_local), jnp.bfloat16)], axis=0)
    outgoing = padded[token_table].reshape(experts, capacity, cols_local)
    arrived = lax.all_to_all(outgoing, "sp", split_axis=0, concat_axis=0, tiled=True).reshape(
        arrived_rows, cols_local
    )
    piece = lax.all_gather(arrived, "tp", axis=1, tiled=True)
    gate_val = jnp.dot(piece, gate_local, preferred_element_type=jnp.float32)
    up_val = jnp.dot(piece, up_local, preferred_element_type=jnp.float32)
    hidden = (jax.nn.silu(gate_val) * up_val).astype(jnp.bfloat16)
    down_local = down_weight[0]
    expert_out = jnp.dot(
        lax.all_gather(hidden, "tp", axis=1, tiled=True),
        down_local,
        preferred_element_type=jnp.float32,
    ).astype(jnp.bfloat16)
    returned = lax.all_to_all(
        expert_out.reshape(experts, capacity, cols_local),
        "sp",
        split_axis=0,
        concat_axis=0,
        tiled=True,
    )
    picked = (
        returned.reshape(arrived_rows, cols_local)[slot_index]
        .reshape(row_count, 2, cols_local)
        .astype(jnp.float32)
    )
    mix_weight = (
        group_weight[:, None] * expert_weight / jnp.sum(expert_weight, axis=1, keepdims=True)
    )
    routed_sum = jnp.sum(picked * mix_weight[:, :, None], axis=1)
    return (resid_wide + routed_sum).astype(jnp.bfloat16)


def solution(mesh):
    return jax.shard_map(
        per_device,
        mesh=mesh,
        in_specs=(
            P("sp", "tp"),
            P("sp", "tp"),
            P("sp", "tp"),
            P(None, "tp"),
            P("sp"),
            P(None, "tp"),
            P("sp", "tp"),
            P("tp"),
            P("sp", None),
            P("sp"),
            P("sp", None),
            P("sp", None, "tp"),
            P("sp", None, "tp"),
            P("sp", None, "tp"),
        ),
        out_specs=P("sp", "tp"),
        check_vma=False,
    )
```

profile of v0, /device:TPU:0, one launch (start us, length us, event | category | flops | bytes accessed | tf_op | source)
XLA Modules:
  0.0 289.8 jit_solution(11334027933683522117)
XLA Ops:
  6.5 0.7 convert_element_type.60
  7.3 4.9 %collective-permute-start = (f32[2]{0:T(128)S(1)}, f32[2]{0:T(128)S(1)}, u32[]{:S(2)}, u32[]{:S(2)}) collective-permute-start(f32[2]{0:T(128)S(1)} %slice.34), channel_id=1, source_target_pairs={{0,4},{4,8},{8,12},{12,16},{16,20},{20,24},{24,28},{1,5},{5,9},{9,... | collective-permute-start | bytes 32 | tf_op jit(solution)/shard_map/ppermute | solution.py:12
  12.2 1.1 convert_multiply_fusion.2
  13.3 3.5 %collective-permute-start.1 = (f32[2,512]{1,0:T(2,128)S(1)}, f32[2,512]{1,0:T(2,128)S(1)}, u32[]{:S(2)}, u32[]{:S(2)}) collective-permute-start(f32[2,512]{1,0:T(2,128)S(1)} %slice.50), channel_id=1, source_target_pairs={{0,4},{4,8},{8,12},{12,16},{16,20},{20,24},{24,28},{1,5},{5,9},{9,... | collective-permute-start | bytes 12296 | tf_op jit(solution)/shard_map/ppermute | solution.py:12
  16.7 0.8 fusion.34
  17.6 0.8 slice_compare_fusion.1
  18.4 1.9 fusion.22
  20.4 0.8 copy.17
  21.5 0.7 convert_element_type.64
  22.2 1.1 reduce-window.6
  23.3 0.2 slice_reduce_fusion
  23.6 0.7 broadcast_multiply_fusion
  24.3 0.1 copy.16
  24.7 2.4 scatter_custom_fusion
  27.1 11.7 %all-gather.4.cloned.1.call-done = bf16[256,2048]{1,0:T(8,128)(2,1)} async-done(((bf16[256,512]{1,0:T(8,128)(2,1)}), bf16[256,2048]{1,0:T(8,128)(2,1)}) %all-gather.4.cloned.1.call-update) | async-done | bytes 1048592 | tf_op jit(solution)/shard_map/all_gather | solution.py:48
  38.8 4.0 %fusion.12 = (f32[256]{0:T(256)S(1)}, bf16[256,1024]{1,0:T(8,128)(2,1)S(1)}) fusion(bf16[256,2048]{1,0:T(8,128)(2,1)} %all-gather.4.cloned.1.call-done, bf16[2048,1024]{1,0:T(8,128)(2,1)} %param.19, bf16[256,1024]{1,0:T(8,128)(2,1)} %param.20), kind=kOutput, calls=%fused_computation.17 | convolution fusion | flops 1075314432 | bytes 6292480 | tf_op jit(solution)/shard_map/dot_general | solution.py:47
  42.8 5.9 %psum.7 = f32[256]{0:T(256)S(1)} all-reduce(f32[256]{0:T(256)S(1)} %get-tuple-element.10), channel_id=1, replica_groups=mesh['sp'=8,'tp'=4] {'tp'}, use_global_device_ids=true, to_apply=%region_1.2 | all-reduce | flops 256 | bytes 2048 | tf_op jit(solution)/shard_map/psum | solution.py:54
  48.7 0.2 fusion.14
  48.9 4.1 %gather_fusion = bf16[1024,1024]{1,0:T(8,128)(2,1)S(1)} fusion(bf16[257,1024]{1,0:T(8,128)(2,1)S(1)} %concatenate.11, s32[1024]{0:T(1024)S(1)} %fusion.28), kind=kCustom, calls=%fused_computation | custom fusion | bytes 4198400 | tf_op jit(solution)/shard_map/gather | solution.py:72
  53.0 53.6 %all_to_all.10 = bf16[8,128,1024]{2,1,0:T(8,128)(2,1)} all-to-all(bf16[8,128,1024]{2,1,0:T(8,128)(2,1)S(1)} %bitcast.36), channel_id=1, replica_groups=mesh['sp'=8,'tp'=4] {'sp'}, dimensions={0} | all-to-all | bytes 4194304 | tf_op jit(solution)/shard_map/all_to_all | solution.py:73
  106.6 0.2 all-gather.8.cloned.1.call-start
  106.8 56.2 %all-gather.6.cloned.1.call-done = bf16[1024,4096]{1,0:T(8,128)(2,1)} async-done(((bf16[1024,1024]{1,0:T(8,128)(2,1)}), bf16[1024,4096]{1,0:T(8,128)(2,1)}) %all-gather.6.cloned.1.call-update) | async-done | bytes 8388624 | tf_op jit(solution)/shard_map/all_gather | solution.py:76
  163.0 8.3 %fusion.4 = f32[1024,512]{1,0:T(8,128)S(1)} fusion(bf16[1024,4096]{1,0:T(8,128)(2,1)} %all-gather.6.cloned.1.call-done, bf16[1,4096,512]{2,1,0:T(8,128)(2,1)} %param.25), kind=kOutput, calls=%fused_computation.7 | convolution fusion | flops 4294967296 | bytes 14680064 | tf_op jit(solution)/shard_map/dot_general | solution.py:77
  171.3 5.7 %multiply_convert_fusion = bf16[1024,512]{1,0:T(8,128)(2,1)} fusion(f32[1024,512]{1,0:T(8,128)S(1)} %fusion.4, bf16[1024,4096]{1,0:T(8,128)(2,1)S(1)} %copy-done.3, bf16[1,4096,512]{2,1,0:T(8,128)(2,1)S(1)} %copy-done.4), kind=kOutput, calls=%fused_computation.10 | convolution fusion | flops 4298113024 | bytes 15728640 | tf_op jit(solution)/shard_map/dot_general | solution.py:78
  177.0 34.6 %all-gather.8.cloned.1.call-done = bf16[1024,2048]{1,0:T(8,128)(2,1)} async-done(((bf16[1024,512]{1,0:T(8,128)(2,1)}), bf16[1024,2048]{1,0:T(8,128)(2,1)}) %all-gather.8.cloned.1.call-update) | async-done | bytes 4194320 | tf_op jit(solution)/shard_map/all_gather | solution.py:82
  211.6 9.3 %fusion.6 = bf16[1024,1024]{1,0:T(8,128)(2,1)} fusion(bf16[1024,2048]{1,0:T(8,128)(2,1)} %all-gather.8.cloned.1.call-done, bf16[1,2048,1024]{2,1,0:T(8,128)(2,1)} %param.27), kind=kOutput, calls=%fused_computation.11 | convolution fusion | flops 4296015872 | bytes 10485760 | tf_op jit(solution)/shard_map/dot_general | solution.py:81
  220.9 5.6 %all-to-all-start.1 = ((bf16[8,128,1024]{2,1,0:T(8,128)(2,1)}), bf16[8,128,1024]{2,1,0:T(8,128)(2,1)S(1)}, u32[]{:S(2)}, u32[]{:S(2)}) async-start(bf16[8,128,1024]{2,1,0:T(8,128)(2,1)} %bitcast.38), calls=%async_computation.1 | async-start | bytes 4194304 | tf_op jit(solution)/shard_map/all_to_all | solution.py:86
  226.8 48.4 %all-to-all-done.1 = bf16[8,128,1024]{2,1,0:T(8,128)(2,1)S(1)} async-done(((bf16[8,128,1024]{2,1,0:T(8,128)(2,1)}), bf16[8,128,1024]{2,1,0:T(8,128)(2,1)S(1)}, u32[]{:S(2)}, u32[]{:S(2)}) %all-to-all-start.1) | async-done | bytes 2097184 | tf_op jit(solution)/shard_map/all_to_all | solution.py:86
  275.2 2.0 gather_fusion.1
  277.3 1.3 reshape.73
  278.6 2.6 multiply_reduce_fusion
  281.3 2.0 fusion.15
  (36 shorter events, 1.1 us)
Async XLA Ops:
  6.5 32.3 %all-gather.4.cloned.1.call-start = ((), (), s32[]{:S(2)}) async-start(), calls=%async_computation.2 | async-start | bytes 1310720 | tf_op jit(solution)/shard_map/all_gather | solution.py:48
  7.3 10.3 %collective-permute-start = (f32[2]{0:T(128)S(1)}, f32[2]{0:T(128)S(1)}, u32[]{:S(2)}, u32[]{:S(2)}) collective-permute-start(f32[2]{0:T(128)S(1)} %slice.34), channel_id=1, source_target_pairs={{0,4},{4,8},{8,12},{12,16},{16,20},{20,24},{24,28},{1,5},{5,9},{9,... | collective-permute-start | bytes 32 | tf_op jit(solution)/shard_map/ppermute | solution.py:12
  13.3 5.1 %collective-permute-start.1 = (f32[2,512]{1,0:T(2,128)S(1)}, f32[2,512]{1,0:T(2,128)S(1)}, u32[]{:S(2)}, u32[]{:S(2)}) collective-permute-start(f32[2,512]{1,0:T(2,128)S(1)} %slice.50), channel_id=1, source_target_pairs={{0,4},{4,8},{8,12},{12,16},{16,20},{20,24},{24,28},{1,5},{5,9},{9,... | collective-permute-start | bytes 12296 | tf_op jit(solution)/shard_map/ppermute | solution.py:12
  20.3 142.7 %all-gather.6.cloned.1.call-start = ((), (), s32[]{:S(2)}) async-start(), calls=%async_computation.3 | async-start | bytes 10485760 | tf_op jit(solution)/shard_map/all_gather | solution.py:76
  42.8 6.1 %copy-start = (bf16[256,1024]{1,0:T(8,128)(2,1)}, bf16[256,1024]{1,0:T(8,128)(2,1)S(1)}, u32[]{:S(2)}) copy-start(bf16[256,1024]{1,0:T(8,128)(2,1)S(1)} %get-tuple-element.11) | copy-start | bytes 1572868
  106.6 105.0 %all-gather.8.cloned.1.call-start = ((), (), s32[]{:S(2)}) async-start(), calls=%async_computation.4 | async-start | bytes 5242880 | tf_op jit(solution)/shard_map/all_gather | solution.py:82
  163.0 8.3 %copy-start.3 = (bf16[1024,4096]{1,0:T(8,128)(2,1)S(1)}, bf16[1024,4096]{1,0:T(8,128)(2,1)}, u32[]{:S(2)}) copy-start(bf16[1024,4096]{1,0:T(8,128)(2,1)} %all-gather.6.cloned.1.call-done) | copy-start | bytes 25165828
  163.0 8.3 %copy-start.4 = (bf16[1,4096,512]{2,1,0:T(8,128)(2,1)S(1)}, bf16[1,4096,512]{2,1,0:T(8,128)(2,1)}, u32[]{:S(2)}) copy-start(bf16[1,4096,512]{2,1,0:T(8,128)(2,1)} %param.26) | copy-start | bytes 12582916
  220.9 5.6 %copy-start.1 = (f32[256,2]{0,1:T(2,128)S(1)}, f32[256,2]{0,1:T(2,128)}, u32[]{:S(2)}) copy-start(f32[256,2]{0,1:T(2,128)} %param.24) | copy-start | bytes 6148
  220.9 5.7 %copy-start.2 = (f32[256]{0:T(256)S(1)}, f32[256]{0:T(256)}, u32[]{:S(2)}) copy-start(f32[256]{0:T(256)} %param.23) | copy-start | bytes 3076
  220.9 54.3 %all-to-all-start.1 = ((bf16[8,128,1024]{2,1,0:T(8,128)(2,1)}), bf16[8,128,1024]{2,1,0:T(8,128)(2,1)S(1)}, u32[]{:S(2)}, u32[]{:S(2)}) async-start(bf16[8,128,1024]{2,1,0:T(8,128)(2,1)} %bitcast.38), calls=%async_computation.1 | async-start | bytes 4194304 | tf_op jit(solution)/shard_map/all_to_all | solution.py:86
Sparse Core Ops, SparseCore 0:
  20.4 18.3 all-gather.3
  106.7 56.2 all-gather.5
  177.1 34.4 all-gather.7
where the time goes:
time: 290 us
  waiting for transfers between devices  151 us (52%)
  blocking collectives  59.4 us (20%)
  matrix products  27.2 us (9%)
  starting transfers between devices  14.2 us (5%)
  between operations  13.3 us (5%)
  local copies, waits for them, and re-layouts  12.6 us (4%)
  other arithmetic  12.1 us (4%)
    all_gather x1, waiting for transfers between devices, per_device(): piece = lax.all_gather(arrived, 'tp', axis=1, tiled=True)  56.2 us
    all_to_all x1, blocking collectives, per_device(): lax.all_to_all(outgoing, 'sp', split_axis=0, concat_axis=0, tiled=True)  53.6 us
    all_to_all x1, waiting for transfers between devices, per_device(): lax.all_to_all(expert_out.reshape(experts, capacity, cols_local), 'sp', s...  48.4 us
    all_gather x1, waiting for transfers between devices, per_device(): lax.all_gather(hidden, 'tp', axis=1, tiled=True)  34.6 us
    all_gather x1, waiting for transfers between devices, per_device(): lax.all_gather(branch, 'tp', axis=1, tiled=True)  11.7 us
    dot_general x1, matrix products, per_device(): jnp.dot(lax.all_gather(hidden, 'tp', axis=1, tiled=True), down_local, pre...  9.28 us
    ppermute x2, starting transfers between devices, passed_along(): lax.ppermute(value, axis, [(source, source + steps) for source in range(i...  8.32 us
    dot_general x1, matrix products, per_device(): gate_val = jnp.dot(piece, gate_local, preferred_element_type=jnp.float32)  8.27 us
  transfers between devices with their start and end apart: 6, of which 4 were waited for; matrix products, arithmetic and copies ran while one was open for 3% of the time, Pallas kernels for 0%

commit v1 on v0

--- a/solution.py
+++ b/solution.py
@@ -1,9 +1,303 @@
+import functools
+
 import jax
 import jax.numpy as jnp
 from jax import lax
+from jax.experimental import pallas as pl
+from jax.experimental.pallas import tpu as pltpu
 from jax.sharding import PartitionSpec as P
 
 EPS = 1e-06
+MESH = pl.DeviceIdType.MESH
+
+
+def remote(src, dst, send_sem, recv_sem, device):
+    return pltpu.make_async_remote_copy(
+        src_ref=src,
+        dst_ref=dst,
+        send_sem=send_sem,
+        recv_sem=recv_sem,
+        device_id=device,
+        device_id_type=MESH,
+    )
+
+
+def expert_kernel(
+    n,
+    tp,
+    out_ref,
+    gate_hbm,
+    up_hbm,
+    down_hbm,
+    ret_ref,
+    piece,
+    hid,
+    eo,
+    gate_w,
+    up_w,
+    down_w,
+    w_sem,
+    own_sem,
+    a_send,
+    a_recv,
+    y_send,
+    y_recv,
+    p_send,
+    p_recv,
+    hy_send,
+    hy_recv,
+    hp_send,
+    hp_recv,
+    r_send,
+    r_recv,
+):
+    me = lax.axis_index("sp")
+    t = lax.axis_index("tp")
+    chips = tp // 2
+    y, core = lax.div(t, 2), lax.rem(t, 2)
+    partner = t + 1 - 2 * core
+    cap, cols = out_ref.shape[1], out_ref.shape[2]
+    ffn_local = gate_w.shape[1]
+    groups, group_rows = hid.shape[0], hid.shape[1]
+    fans = p_send.shape[1]
+    fan_blocks = n // fans
+    group_fans = fans // groups
+    group_blocks = n // groups
+
+    def column(index, width):
+        return pl.ds(pl.multiple_of(index * width, 128), width)
+
+    def chip_at(delta):
+        return lax.rem(y + delta + chips, chips) * 2 + core
+
+    weight_copies = [
+        pltpu.make_async_copy(source.at[0], target, w_sem.at[i])
+        for i, (source, target) in enumerate(
+            ((gate_hbm, gate_w), (up_hbm, up_w), (down_hbm, down_w))
+        )
+    ]
+    for copy in weight_copies:
+        copy.start()
+
+    barrier = pltpu.get_barrier_semaphore()
+    for k in range(1, n):
+        pl.semaphore_signal(
+            barrier, inc=1, device_id=(lax.rem(me + k, n), t), device_id_type=MESH
+        )
+    pl.semaphore_signal(barrier, inc=1, device_id=(me, partner), device_id_type=MESH)
+    for d in range(1, chips):
+        pl.semaphore_signal(barrier, inc=1, device_id=(me, chip_at(d)), device_id_type=MESH)
+    pl.semaphore_wait(barrier, n - 1 + chips)
+
+    own_in = pltpu.make_async_copy(out_ref.at[me], piece.at[0, :, column(t, cols)], own_sem.at[0])
+    own_in.start()
+    sends = []
+    arrivals = []
+    for k in range(1, n):
+        there = lax.rem(me + k, n)
+        copy = remote(
+            out_ref.at[there],
+            piece.at[k, :, column(t, cols)],
+            a_send.at[k],
+            a_recv.at[k],
+            (there, t),
+        )
+        copy.start()
+        sends.append(copy)
+        arrivals.append(copy)
+
+    def fan_region(f, index):
+        return piece.at[pl.ds(f * fan_blocks, fan_blocks), :, column(index, cols)]
+
+    def fan_out(f):
+        for k in range(f * fan_blocks, (f + 1) * fan_blocks):
+            if k == 0:
+                own_in.wait()
+            else:
+                arrivals[k - 1].wait_recv()
+        region = fan_region(f, t)
+        for d in range(1, chips):
+            copy = remote(
+                region, region, y_send.at[d, f], y_recv.at[d, f], (me, chip_at(d))
+            )
+            copy.start()
+            sends.append(copy)
+        copy = remote(region, region, p_send.at[0, f], p_recv.at[0, f], (me, partner))
+        copy.start()
+        sends.append(copy)
+
+    def relay(f):
+        for d in range(1, chips):
+            source = chip_at(-d)
+            region = fan_region(f, source)
+            remote(
+                region, region, y_send.at[d, f], y_recv.at[d, f], (me, partner)
+            ).wait_recv()
+            copy = remote(region, region, p_send.at[d, f], p_recv.at[d, f], (me, partner))
+            copy.start()
+            sends.append(copy)
+
+    def hid_region(g, index):
+        return hid.at[g, :, column(index, ffn_local)]
+
+    def up_stage(g):
+        for f in range(g * group_fans, (g + 1) * group_fans):
+            for d in range(chips):
+                region = fan_region(f, chip_at(-d) + partner - t)
+                remote(
+                    region, region, p_send.at[d, f], p_recv.at[d, f], (me, partner)
+                ).wait_recv()
+        if g == 0:
+            weight_copies[0].wait()
+            weight_copies[1].wait()
+        step = min(256, ffn_local)
+
+        def tile(j, carry):
+            rows = piece[pl.ds(g * group_blocks, group_blocks)].reshape(group_rows, tp * cols)
+            at = pl.ds(pl.multiple_of(j * step, 128), step)
+            gate_val = jnp.dot(rows, gate_w[:, at], preferred_element_type=jnp.float32)
+            up_val = jnp.dot(rows, up_w[:, at], preferred_element_type=jnp.float32)
+            hidden = (jax.nn.silu(gate_val) * up_val).astype(jnp.bfloat16)
+            hid[g, :, pl.ds(pl.multiple_of(t * ffn_local + j * step, 128), step)] = hidden
+            return carry
+
+        lax.fori_loop(0, ffn_local // step, tile, 0)
+        region = hid_region(g, t)
+        for d in range(1, chips):
+            copy = remote(
+                region, region, hy_send.at[d, g], hy_recv.at[d, g], (me, chip_at(d))
+            )
+            copy.start()
+            sends.append(copy)
+        copy = remote(region, region, hp_send.at[0, g], hp_recv.at[0, g], (me, partner))
+        copy.start()
+        sends.append(copy)
+
+    def relay_hidden(g):
+        for d in range(1, chips):
+            region = hid_region(g, chip_at(-d))
+            remote(
+                region, region, hy_send.at[d, g], hy_recv.at[d, g], (me, partner)
+            ).wait_recv()
+            copy = remote(region, region, hp_send.at[d, g], hp_recv.at[d, g], (me, partner))
+            copy.start()
+            sends.append(copy)
+
+    returns = []
+
+    def down_stage(g):
+        for d in range(chips):
+            region = hid_region(g, chip_at(-d) + partner - t)
+            remote(
+                region, region, hp_send.at[d, g], hp_recv.at[d, g], (me, partner)
+            ).wait_recv()
+        if g == 0:
+            weight_copies[2].wait()
+        step = min(256, cols)
+
+        def tile(j, carry):
+            at = pl.ds(pl.multiple_of(j * step, 128), step)
+            value = jnp.dot(hid[g], down_w[:, at], preferred_element_type=jnp.float32)
+            eo[pl.ds(g * group_blocks, group_blocks), :, at] = value.astype(
+                jnp.bfloat16
+            ).reshape(group_blocks, cap, step)
+            return carry
+
+        lax.fori_loop(0, cols // step, tile, 0)
+        for k in range(g * group_blocks, (g + 1) * group_blocks):
+            if k == 0:
+                copy = pltpu.make_async_copy(eo.at[0], ret_ref.at[me], own_sem.at[1])
+            else:
+                copy = remote(
+                    eo.at[k],
+                    ret_ref.at[me],
+                    r_send.at[k],
+                    r_recv.at[k],
+                    (lax.rem(me + n - k, n), t),
+                )
+            copy.start()
+            returns.append(copy)
+
+    def fans_of(g):
+        return range(g * group_fans, (g + 1) * group_fans)
+
+    ahead = min(2, groups)
+    for g in range(ahead):
+        for f in fans_of(g):
+            fan_out(f)
+    for g in range(groups):
+        for f in fans_of(g):
+            relay(f)
+        up_stage(g)
+        if g + ahead < groups:
+            for f in fans_of(g + ahead):
+                fan_out(f)
+        if g >= 1:
+            relay_hidden(g - 1)
+            down_stage(g - 1)
+    relay_hidden(groups - 1)
+    down_stage(groups - 1)
+
+    for k, copy in enumerate(returns):
+        if k == 0:
+            copy.wait()
+        else:
+            there = lax.rem(me + k, n)
+            copy.wait_send()
+            remote(
+                eo.at[k], ret_ref.at[there], r_send.at[k], r_recv.at[k], (there, t)
+            ).wait_recv()
+    for copy in sends:
+        copy.wait_send()
+
+
+def expert_layer(outgoing, gate_weight, up_weight, down_weight):
+    n, tp = lax.axis_size("sp"), lax.axis_size("tp")
+    cap, cols = outgoing.shape[1], outgoing.shape[2]
+    chips = tp // 2
+    rows = n * cap
+    groups = max(1, min(4, rows // 256))
+    fans = min(n, 2 * groups)
+    width, ffn_local = gate_weight.shape[1], gate_weight.shape[2]
+    ffn = down_weight.shape[1]
+    dma = pltpu.SemaphoreType.DMA
+    flops = 2 * rows * width * ffn_local * 2 + 2 * rows * ffn * cols
+    return pl.pallas_call(
+        functools.partial(expert_kernel, n, tp),
+        out_shape=jax.ShapeDtypeStruct(outgoing.shape, jnp.bfloat16),
+        in_specs=[pl.BlockSpec(memory_space=pltpu.VMEM)]
+        + [pl.BlockSpec(memory_space=pl.ANY)] * 3,
+        out_specs=pl.BlockSpec(memory_space=pltpu.VMEM),
+        scratch_shapes=[
+            pltpu.VMEM((n, cap, width), jnp.bfloat16),
+            pltpu.VMEM((groups, rows // groups, ffn), jnp.bfloat16),
+            pltpu.VMEM((n, cap, cols), jnp.bfloat16),
+            pltpu.VMEM((width, ffn_local), jnp.bfloat16),
+            pltpu.VMEM((width, ffn_local), jnp.bfloat16),
+            pltpu.VMEM((ffn, cols), jnp.bfloat16),
+            dma((3,)),
+            dma((2,)),
+            dma((n,)),
+            dma((n,)),
+            dma((chips, fans)),
+            dma((chips, fans)),
+            dma((chips, fans)),
+            dma((chips, fans)),
+            dma((chips, groups)),
+            dma((chips, groups)),
+            dma((chips, groups)),
+            dma((chips, groups)),
+            dma((n,)),
+            dma((n,)),
+        ],
+        compiler_params=pltpu.CompilerParams(
+            collective_id=0, has_side_effects=True, vmem_limit_bytes=48 * 1024 * 1024
+        ),
+        cost_estimate=pl.CostEstimate(
+            flops=flops, bytes_accessed=3 * width * ffn_local * 2, transcendentals=0
+        ),
+        name="experts",
+    )(outgoing, gate_weight, up_weight, down_weight)
 
 
 def passed_along(value, axis, steps):
@@ -63,33 +357,18 @@
     )
     slot_rank = jnp.sum((jnp.cumsum(onehot, axis=0) - onehot) * onehot, axis=1)
     slot_index = flat_experts * capacity + slot_rank
-    token_of = jnp.arange(2 * row_count, dtype=jnp.int32) // 2
-    token_table = jnp.full((experts * capacity,), row_count, jnp.int32).at[slot_index].set(token_of)
-    gate_local = gate_weight[0]
-    up_local = up_weight[0]
+    slots = slot_index.reshape(row_count, 2)
     arrived_rows = experts * capacity
-    padded = jnp.concatenate([normed, jnp.zeros((1, cols_local), jnp.bfloat16)], axis=0)
-    outgoing = padded[token_table].reshape(experts, capacity, cols_local)
-    arrived = lax.all_to_all(outgoing, "sp", split_axis=0, concat_axis=0, tiled=True).reshape(
-        arrived_rows, cols_local
-    )
-    piece = lax.all_gather(arrived, "tp", axis=1, tiled=True)
-    gate_val = jnp.dot(piece, gate_local, preferred_element_type=jnp.float32)
-    up_val = jnp.dot(piece, up_local, preferred_element_type=jnp.float32)
-    hidden = (jax.nn.silu(gate_val) * up_val).astype(jnp.bfloat16)
-    down_local = down_weight[0]
-    expert_out = jnp.dot(
-        lax.all_gather(hidden, "tp", axis=1, tiled=True),
-        down_local,
-        preferred_element_type=jnp.float32,
+    slot_iota = jnp.arange(arrived_rows, dtype=jnp.int32)[:, None]
+    select = (
+        (slot_iota == slots[:, 0][None, :]) | (slot_iota == slots[:, 1][None, :])
     ).astype(jnp.bfloat16)
-    returned = lax.all_to_all(
-        expert_out.reshape(experts, capacity, cols_local),
-        "sp",
-        split_axis=0,
-        concat_axis=0,
-        tiled=True,
-    )
+    outgoing = (
+        jnp.dot(select, normed, preferred_element_type=jnp.float32)
+        .astype(jnp.bfloat16)
+        .reshape(experts, capacity, cols_local)
+    )
+    returned = expert_layer(outgoing, gate_weight, up_weight, down_weight)
     picked = (
         returned.reshape(arrived_rows, cols_local)[slot_index]
         .reshape(row_count, 2, cols_local)

time: 290 us -> 190 us (0.66)
  waiting for transfers between devices: 151 us -> 13.1 us
  Pallas kernels: 0 us -> 125 us
  blocking collectives: 59.4 us -> 6.06 us
  matrix products: 27.2 us -> 4.82 us
  local copies, waits for them, and re-layouts: 12.6 us -> 6.24 us
  starting transfers between devices: 14.2 us -> 8.32 us
    pallas_call x0 -> x1, Pallas kernels: none -> 125 us  [expert_layer(): pl.pallas_call(functools.partial(expert_kernel, n, tp), out_shape=jax.Sha...]
    all_gather x2 -> x0, waiting for transfers between devices: 90.8 us -> none  [the longest x1 56.2 us: per_device(): piece = lax.all_gather(arrived, 'tp', axis=1, tiled=True)]
    all_to_all x1 -> x0, blocking collectives: 53.6 us -> none  [per_device(): lax.all_to_all(outgoing, 'sp', split_axis=0, concat_axis=0, tiled=True)]
    all_to_all x1 -> x0, waiting for transfers between devices: 48.4 us -> none  [per_device(): lax.all_to_all(expert_out.reshape(experts, capacity, cols_local), 'sp', s...]
    dot_general x3 -> x1, matrix products: 23.3 us -> 0.84 us  [per_device(): jnp.dot(select, normed, preferred_element_type=jnp.float32)]
    all_to_all x1 -> x0, starting transfers between devices: 5.64 us -> none  [per_device(): lax.all_to_all(expert_out.reshape(experts, capacity, cols_local), 'sp', s...]
    gather x1 -> x0, local copies, waits for them, and re-layouts: 4.07 us -> none  [per_device(): outgoing = padded[token_table].reshape(experts, capacity, cols_local)]
  transfers between devices with their start and end apart: 6 -> 3, of which waited for: 4 -> 1; matrix products, arithmetic and copies ran while one was open for 3% -> 4% of each run, Pallas kernels for 0% -> 0%
where the time goes in v1:
time: 190 us; the launch traced here: 189 us
  Pallas kernels  125 us (66%)
  between operations  13.5 us (7%)
  waiting for transfers between devices  13.1 us (7%)
  other arithmetic  12.6 us (7%)
  starting transfers between devices  8.32 us (4%)
  local copies, waits for them, and re-layouts  6.24 us (3%)
  blocking collectives  6.06 us (3%)
  matrix products  4.82 us (3%)
    pallas_call x1, Pallas kernels, expert_layer(): pl.pallas_call(functools.partial(expert_kernel, n, tp), out_shape=jax.Sha...  125 us
    all_gather x1, waiting for transfers between devices, per_device(): lax.all_gather(branch, 'tp', axis=1, tiled=True)  13.1 us
    ppermute x2, starting transfers between devices, passed_along(): lax.ppermute(value, axis, [(source, source + steps) for source in range(i...  8.32 us
    psum x1, blocking collectives, per_device(): total_sq = lax.psum(jnp.sum(resid_wide * resid_wide, axis=1), 'tp')  6.06 us
    dot_general x1, matrix products, per_device(): jnp.dot(lax.all_gather(branch, 'tp', axis=1, tiled=True), output_weight,...  3.97 us
  transfers between devices with their start and end apart: 3, of which 1 were waited for; matrix products, arithmetic and copies ran while one was open for 4% of the time, Pallas kernels for 0%

profile of v1, /device:TPU:0, one launch (start us, length us, event | category | flops | bytes accessed | tf_op | source)
XLA Modules:
  0.0 189.3 jit_solution(15621978313005024996)
XLA Ops:
  6.5 0.7 convert_element_type.58
  7.2 0.1 slice.40
  7.3 4.9 %collective-permute-start = (f32[2]{0:T(128)S(1)}, f32[2]{0:T(128)S(1)}, u32[]{:S(2)}, u32[]{:S(2)}) collective-permute-start(f32[2]{0:T(128)S(1)} %slice.40), channel_id=1, source_target_pairs={{0,4},{4,8},{8,12},{12,16},{16,20},{20,24},{24,28},{1,5},{5,9},{9,... | collective-permute-start | bytes 32 | tf_op jit(solution)/shard_map/ppermute | solution.py:306
  12.2 1.1 convert_multiply_fusion.2
  13.3 3.5 %collective-permute-start.1 = (f32[2,512]{1,0:T(2,128)S(1)}, f32[2,512]{1,0:T(2,128)S(1)}, u32[]{:S(2)}, u32[]{:S(2)}) collective-permute-start(f32[2,512]{1,0:T(2,128)S(1)} %slice.56), channel_id=1, source_target_pairs={{0,4},{4,8},{8,12},{12,16},{16,20},{20,24},{24,28},{1,5},{5,9},{9,... | collective-permute-start | bytes 12296 | tf_op jit(solution)/shard_map/ppermute | solution.py:306
  16.7 0.8 fusion.25
  17.6 0.1 pad_maximum_fusion.1
  17.6 0.8 slice_compare_fusion.1
  18.4 1.9 %fusion.13 = bf16[256,512]{1,0:T(8,128)(2,1)} fusion(f32[2,512]{1,0:T(2,128)S(1)} %collective-permute-done.1, f32[256,512]{1,0:T(8,128)S(1)} %convert_multiply_fusion.2, bf16[256,512]{1,0:T(8,128)(2,1)} %param.14, f32[512]{0:T(512)S(1)} %bitcast.22, f32[512]{0:T(512)S(1)} %bitcast.21, f32[512]{0:T(512)S(1)} %bitcast.20, ...), kind=kLoop, calls=%fused_computation.23 | loop fusion | flops 1572864 | bytes 1059328 | tf_op jit(solution)/shard_map/convert_element_type | solution.py:339
  20.3 0.0 all-gather.2.cloned.1.call-update
  20.3 0.8 copy.20
  21.1 0.1 eq.68
  21.3 0.1 eq.64
  21.4 1.1 reduce-window.6
  22.6 0.2 slice_reduce_fusion.2
  22.9 0.1 fusion.22
  22.9 0.1 reduce_sum.41
  23.1 0.7 convert_element_type.64
  23.8 0.1 mul.110
  23.9 0.7 reduce_sum.44
  24.6 0.7 multiply_divide_fusion
  25.3 0.1 copy.23
  25.5 0.2 slice_reduce_fusion.1
  25.7 13.1 %all-gather.2.cloned.1.call-done = bf16[256,2048]{1,0:T(8,128)(2,1)} async-done(((bf16[256,512]{1,0:T(8,128)(2,1)}), bf16[256,2048]{1,0:T(8,128)(2,1)}) %all-gather.2.cloned.1.call-update) | async-done | bytes 1048592 | tf_op jit(solution)/shard_map/all_gather | solution.py:342
  38.8 4.0 %fusion.1 = (f32[256]{0:T(256)S(1)}, bf16[256,1024]{1,0:T(8,128)(2,1)S(1)}) fusion(bf16[256,2048]{1,0:T(8,128)(2,1)} %all-gather.2.cloned.1.call-done, bf16[2048,1024]{1,0:T(8,128)(2,1)} %param.19, bf16[256,1024]{1,0:T(8,128)(2,1)} %param.20), kind=kOutput, calls=%fused_computation.8 | convolution fusion | flops 1075314432 | bytes 6292480 | tf_op jit(solution)/shard_map/dot_general | solution.py:341
  42.8 6.1 %psum.7 = f32[256]{0:T(256)S(1)} all-reduce(f32[256]{0:T(256)S(1)} %get-tuple-element.14), channel_id=1, replica_groups=mesh['sp'=8,'tp'=4] {'tp'}, use_global_device_ids=true, to_apply=%region_4.5 | all-reduce | flops 256 | bytes 2048 | tf_op jit(solution)/shard_map/psum | solution.py:348
  48.9 0.8 convolution_convert_fusion
  49.7 124.7 %experts.1 = bf16[8,128,1024]{2,1,0:T(8,128)(2,1)S(1)} custom-call(bf16[8,128,1024]{2,1,0:T(8,128)(2,1)S(1)} %bitcast.18, bf16[1,4096,512]{2,1,0:T(8,128)(2,1)} %gate_hbm.1, bf16[1,4096,512]{2,1,0:T(8,128)(2,1)} %up_hbm.1, bf16[1,2048,1024]{2,1,0:T(8,128)(2,1)} %down_hbm.1), custom_call_target="tpu_custom_call" | custom-call | flops 12884901888 | bytes 12582912 | tf_op jit(solution)/shard_map/experts/pallas_call | solution.py:265
  174.4 2.1 %gather_fusion = bf16[512,1024]{1,0:T(8,128)(2,1)S(1)} fusion(bf16[1024,1024]{1,0:T(8,128)(2,1)S(1)} %bitcast.17, s32[1024]{0:T(1024)S(1)} %pad_clamp_fusion), kind=kCustom, calls=%fused_computation | custom fusion | bytes 2099200 | tf_op jit(solution)/shard_map/gather | solution.py:373
  176.5 1.3 reshape.69
  177.8 2.6 %multiply_reduce_fusion = f32[256,1024]{1,0:T(8,128)S(1)} fusion(f32[256,2,1024]{2,1,0:T(2,128)S(1)} %reshape.69, f32[256,2]{1,0:T(8,128)S(1)} %copy.23), kind=kLoop, calls=%fused_computation.1 | loop fusion | flops 786432 | bytes 3147776 | tf_op jit(solution)/shard_map/reduce_sum | solution.py:380
  180.5 2.0 %fusion.4 = bf16[256,1024]{1,0:T(8,128)(2,1)} fusion(f32[256,1024]{1,0:T(8,128)S(1)} %multiply_reduce_fusion, bf16[256,1024]{1,0:T(8,128)(2,1)} %copy-done), kind=kLoop, calls=%fused_computation.11 | loop fusion | flops 786432 | bytes 2097152 | tf_op jit(solution)/shard_map/convert_element_type | solution.py:381
  (13 shorter events, 0.1 us)
Async XLA Ops:
  6.5 32.3 %all-gather.2.cloned.1.call-start = ((), (), s32[]{:S(2)}) async-start(), calls=%async_computation | async-start | bytes 1310720 | tf_op jit(solution)/shard_map/all_gather | solution.py:342
  7.3 10.3 %collective-permute-start = (f32[2]{0:T(128)S(1)}, f32[2]{0:T(128)S(1)}, u32[]{:S(2)}, u32[]{:S(2)}) collective-permute-start(f32[2]{0:T(128)S(1)} %slice.40), channel_id=1, source_target_pairs={{0,4},{4,8},{8,12},{12,16},{16,20},{20,24},{24,28},{1,5},{5,9},{9,... | collective-permute-start | bytes 32 | tf_op jit(solution)/shard_map/ppermute | solution.py:306
  13.3 5.1 %collective-permute-start.1 = (f32[2,512]{1,0:T(2,128)S(1)}, f32[2,512]{1,0:T(2,128)S(1)}, u32[]{:S(2)}, u32[]{:S(2)}) collective-permute-start(f32[2,512]{1,0:T(2,128)S(1)} %slice.56), channel_id=1, source_target_pairs={{0,4},{4,8},{8,12},{12,16},{16,20},{20,24},{24,28},{1,5},{5,9},{9,... | collective-permute-start | bytes 12296 | tf_op jit(solution)/shard_map/ppermute | solution.py:306
  42.8 6.9 %copy-start = (bf16[256,1024]{1,0:T(8,128)(2,1)}, bf16[256,1024]{1,0:T(8,128)(2,1)S(1)}, u32[]{:S(2)}) copy-start(bf16[256,1024]{1,0:T(8,128)(2,1)S(1)} %get-tuple-element.15) | copy-start | bytes 1572868
Sparse Core Ops, SparseCore 0:
  20.4 18.3 all-gather.1

commit v2 on v1

--- a/solution.py
+++ b/solution.py
@@ -25,11 +25,34 @@
 def expert_kernel(
     n,
     tp,
-    out_ref,
+    outer_ref,
+    inner_ref,
+    conv_ref,
+    taps_ref,
+    docs_ref,
+    residual_ref,
+    gain_ref,
+    ids_ref,
+    mix_ref,
+    proj_hbm,
     gate_hbm,
     up_hbm,
     down_hbm,
+    result_ref,
+    out_ref,
     ret_ref,
+    branch,
+    proj_w,
+    acc,
+    resid,
+    normed,
+    squares,
+    key_col,
+    key_row,
+    mix_col,
+    halo_inner,
+    halo_conv,
+    halo_docs,
     piece,
     hid,
     eo,
@@ -50,6 +73,14 @@
     hp_recv,
     r_send,
     r_recv,
+    h_send,
+    h_recv,
+    by_send,
+    by_recv,
+    bp_send,
+    bp_recv,
+    s_send,
+    s_recv,
 ):
     me = lax.axis_index("sp")
     t = lax.axis_index("tp")
@@ -71,30 +102,192 @@
         return lax.rem(y + delta + chips, chips) * 2 + core
 
     weight_copies = [
-        pltpu.make_async_copy(source.at[0], target, w_sem.at[i])
+        pltpu.make_async_copy(source, target, w_sem.at[i])
         for i, (source, target) in enumerate(
-            ((gate_hbm, gate_w), (up_hbm, up_w), (down_hbm, down_w))
+            (
+                (gate_hbm.at[0], gate_w),
+                (up_hbm.at[0], up_w),
+                (down_hbm.at[0], down_w),
+                (proj_hbm, proj_w),
+            )
         )
     ]
-    for copy in weight_copies:
-        copy.start()
+    for i in (3, 0, 1, 2):
+        weight_copies[i].start()
 
     barrier = pltpu.get_barrier_semaphore()
     for k in range(1, n):
         pl.semaphore_signal(
             barrier, inc=1, device_id=(lax.rem(me + k, n), t), device_id_type=MESH
         )
-    pl.semaphore_signal(barrier, inc=1, device_id=(me, partner), device_id_type=MESH)
-    for d in range(1, chips):
-        pl.semaphore_signal(barrier, inc=1, device_id=(me, chip_at(d)), device_id_type=MESH)
-    pl.semaphore_wait(barrier, n - 1 + chips)
-
-    own_in = pltpu.make_async_copy(out_ref.at[me], piece.at[0, :, column(t, cols)], own_sem.at[0])
-    own_in.start()
+    for d in range(1, tp):
+        pl.semaphore_signal(
+            barrier, inc=1, device_id=(me, lax.rem(t + d, tp)), device_id_type=MESH
+        )
+    pl.semaphore_wait(barrier, n - 1 + tp - 1)
+
     sends = []
     arrivals = []
+    row_count = residual_ref.shape[0]
+    wide = branch.shape[1] // tp
+
+    halos = []
+    following = (lax.rem(me + 1, n), t)
+    for i, (source, target) in enumerate(
+        (
+            (inner_ref.at[pl.ds(row_count - 16, 16)], halo_inner),
+            (conv_ref.at[pl.ds(row_count - 16, 16)], halo_conv),
+            (docs_ref.at[pl.ds(row_count - 8, 8)], halo_docs),
+        )
+    ):
+        copy = remote(source, target, h_send.at[i], h_recv.at[i], following)
+        copy.start()
+        halos.append(copy)
+        sends.append(copy)
+
+    lanes = lax.broadcasted_iota(jnp.int32, (row_count, 128), 1)
+    first_id, second_id = ids_ref[:, 0:1], ids_ref[:, 1:2]
+    is_first, is_second = lanes == first_id, lanes == second_id
+    mix_col[...] = jnp.where(is_first, mix_ref[:, 0:1], 0.0) + jnp.where(
+        is_second, mix_ref[:, 1:2], 0.0
+    )
+    member = jnp.where(is_first, 1.0, 0.0) + jnp.where(is_second, 1.0, 0.0)
+    earlier = jnp.where(
+        lax.broadcasted_iota(jnp.int32, (row_count, row_count), 1)
+        < lax.broadcasted_iota(jnp.int32, (row_count, row_count), 0),
+        1.0,
+        0.0,
+    ).astype(jnp.bfloat16)
+    ranks = jnp.dot(earlier, member.astype(jnp.bfloat16), preferred_element_type=jnp.float32)
+    keys = jnp.where(member > 0.5, ranks, -1.0)
+    key_col[...] = keys
+    key_row[...] = keys.T
+
+    for copy in halos:
+        copy.wait_recv()
+    row_at = lax.broadcasted_iota(jnp.int32, (row_count, 1), 0)
+    own_docs = docs_ref[:, 0:1]
+    halo_ids = jnp.where(me > 0, halo_docs[...], -1.0)[:, 0:1]
+    docs_one = jnp.where(row_at == 0, halo_ids[7:8], pltpu.roll(docs_ref[...], 1, 0)[:, 0:1])
+    docs_two = jnp.where(
+        row_at == 0,
+        halo_ids[6:7],
+        jnp.where(row_at == 1, halo_ids[7:8], pltpu.roll(docs_ref[...], 2, 0)[:, 0:1]),
+    )
+    same_one, same_two = docs_one == own_docs, docs_two == own_docs
+
+    def conv_tile(j, carry):
+        at = pl.ds(pl.multiple_of(j * 128, 128), 128)
+        products = inner_ref[:, at].astype(jnp.float32) * conv_ref[:, at].astype(jnp.float32)
+        before = halo_inner[:, at].astype(jnp.float32) * halo_conv[:, at].astype(jnp.float32)
+        one = jnp.where(row_at == 0, before[15:16], pltpu.roll(products, 1, 0))
+        two = jnp.where(
+            row_at == 0,
+            before[14:15],
+            jnp.where(row_at == 1, before[15:16], pltpu.roll(products, 2, 0)),
+        )
+        taps = taps_ref[:, at].astype(jnp.float32)
+        conv = taps[2:3] * products
+        conv = conv + jnp.where(same_one, taps[1:2] * one, 0.0)
+        conv = conv + jnp.where(same_two, taps[0:1] * two, 0.0)
+        value = (outer_ref[:, at].astype(jnp.float32) * conv).astype(jnp.bfloat16)
+        branch[:, pl.ds(pl.multiple_of(t * wide + j * 128, 128), 128)] = value
+        return carry
+
+    lax.fori_loop(0, wide // 128, conv_tile, 0)
+
+    def branch_region(index):
+        return branch.at[:, column(index, wide)]
+
+    region = branch_region(t)
+    for d in range(1, chips):
+        copy = remote(region, region, by_send.at[d], by_recv.at[d], (me, chip_at(d)))
+        copy.start()
+        sends.append(copy)
+    copy = remote(region, region, bp_send.at[0], bp_recv.at[0], (me, partner))
+    copy.start()
+    sends.append(copy)
+    weight_copies[3].wait()
+
+    def project(index, first=False):
+        step = min(256, cols)
+
+        def tile(j, carry):
+            at = pl.ds(pl.multiple_of(j * step, 128), step)
+            rows = pl.ds(pl.multiple_of(index * wide, 128), wide)
+            value = jnp.dot(
+                branch[:, column(index, wide)], proj_w[rows, at], preferred_element_type=jnp.float32
+            )
+            acc[:, at] = value if first else acc[:, at] + value
+            return carry
+
+        lax.fori_loop(0, cols // step, tile, 0)
+
+    project(t, True)
+    other = branch_region(partner)
+    remote(other, other, bp_send.at[0], bp_recv.at[0], (me, partner)).wait_recv()
+    project(partner)
+    for d in range(1, chips):
+        source = chip_at(-d)
+        region = branch_region(source)
+        remote(region, region, by_send.at[d], by_recv.at[d], (me, partner)).wait_recv()
+        copy = remote(region, region, bp_send.at[d], bp_recv.at[d], (me, partner))
+        copy.start()
+        sends.append(copy)
+        project(source)
+    for d in range(1, chips):
+        source = chip_at(-d) + partner - t
+        region = branch_region(source)
+        remote(region, region, bp_send.at[d], bp_recv.at[d], (me, partner)).wait_recv()
+        project(source)
+
+    def resid_tile(j, total):
+        at = pl.ds(pl.multiple_of(j * 128, 128), 128)
+        value = (residual_ref[:, at].astype(jnp.float32) + acc[:, at]).astype(jnp.bfloat16)
+        resid[:, at] = value
+        value = value.astype(jnp.float32)
+        return total + value * value
+
+    total = lax.fori_loop(
+        0, cols // 128, resid_tile, jnp.zeros((row_count, 128), jnp.float32)
+    )
+    squares[t] = jnp.broadcast_to(
+        jnp.sum(total.T, axis=0, keepdims=True), (8, row_count)
+    )
+    for d in range(1, tp):
+        copy = remote(
+            squares.at[t], squares.at[t], s_send.at[d], s_recv.at[d], (me, lax.rem(t + d, tp))
+        )
+        copy.start()
+        sends.append(copy)
+    for d in range(1, tp):
+        source = lax.rem(t + tp - d, tp)
+        remote(
+            squares.at[source], squares.at[source], s_send.at[d], s_recv.at[d], (me, source)
+        ).wait_recv()
+    total_sq = jnp.sum(squares[...], axis=0)[0:1]
+    scale_row = lax.rsqrt(total_sq / (tp * cols) + EPS)
+    scale = jnp.broadcast_to(scale_row, (128, row_count)).T
+
+    def norm_tile(j, carry):
+        at = pl.ds(pl.multiple_of(j * 128, 128), 128)
+        value = resid[:, at].astype(jnp.float32) * scale * gain_ref[:, at].astype(jnp.float32)
+        normed[:, at] = value.astype(jnp.bfloat16)
+        return carry
+
+    lax.fori_loop(0, cols // 128, norm_tile, 0)
+
+    slot_rows = lax.broadcasted_iota(jnp.int32, (cap, row_count), 0).astype(jnp.float32)
+
+    def choose(expert):
+        select = jnp.where(slot_rows == key_row[pl.ds(expert, 1), :], 1.0, 0.0)
+        out_ref[expert] = jnp.dot(
+            select.astype(jnp.bfloat16), normed[...], preferred_element_type=jnp.float32
+        ).astype(jnp.bfloat16)
+
     for k in range(1, n):
         there = lax.rem(me + k, n)
+        choose(there)
         copy = remote(
             out_ref.at[there],
             piece.at[k, :, column(t, cols)],
@@ -105,6 +298,9 @@
         copy.start()
         sends.append(copy)
         arrivals.append(copy)
+    choose(me)
+    own_in = pltpu.make_async_copy(out_ref.at[me], piece.at[0, :, column(t, cols)], own_sem.at[0])
+    own_in.start()
 
     def fan_region(f, index):
         return piece.at[pl.ds(f * fan_blocks, fan_blocks), :, column(index, cols)]
@@ -238,44 +434,89 @@
     relay_hidden(groups - 1)
     down_stage(groups - 1)
 
-    for k, copy in enumerate(returns):
-        if k == 0:
-            copy.wait()
-        else:
+    slot_lanes = lax.broadcasted_iota(jnp.int32, (row_count, cap), 1).astype(jnp.float32)
+    for g in range(groups):
+        members = range(g * group_blocks, (g + 1) * group_blocks)
+        for k in members:
+            if k == 0:
+                returns[0].wait()
+            else:
+                there = lax.rem(me + k, n)
+                returns[k].wait_send()
+                remote(
+                    eo.at[k], ret_ref.at[there], r_send.at[k], r_recv.at[k], (there, t)
+                ).wait_recv()
+        chosen = []
+        for k in members:
             there = lax.rem(me + k, n)
-            copy.wait_send()
-            remote(
-                eo.at[k], ret_ref.at[there], r_send.at[k], r_recv.at[k], (there, t)
-            ).wait_recv()
+            here = lanes == there
+            key = jnp.sum(jnp.where(here, key_col[...], 0.0), axis=1, keepdims=True)
+            weight = jnp.sum(jnp.where(here, mix_col[...], 0.0), axis=1, keepdims=True)
+            select = jnp.where(slot_lanes == key, 1.0, 0.0).astype(jnp.bfloat16)
+            chosen.append((there, select, weight))
+        step = min(256, cols)
+
+        def combine(j, carry):
+            at = pl.ds(pl.multiple_of(j * step, 128), step)
+            value = jnp.zeros((row_count, step), jnp.float32) if g == 0 else acc[:, at]
+            for there, select, weight in chosen:
+                value = value + weight * jnp.dot(
+                    select, ret_ref[there, :, at], preferred_element_type=jnp.float32
+                )
+            if g == groups - 1:
+                result_ref[:, at] = (resid[:, at].astype(jnp.float32) + value).astype(jnp.bfloat16)
+            else:
+                acc[:, at] = value
+            return carry
+
+        lax.fori_loop(0, cols // step, combine, 0)
     for copy in sends:
         copy.wait_send()
 
 
-def expert_layer(outgoing, gate_weight, up_weight, down_weight):
+def whole_layer(blocks, weights):
     n, tp = lax.axis_size("sp"), lax.axis_size("tp")
-    cap, cols = outgoing.shape[1], outgoing.shape[2]
+    row_count, wide = blocks[0].shape
+    cols = blocks[5].shape[1]
+    cap = 4 * row_count // n
     chips = tp // 2
     rows = n * cap
     groups = max(1, min(4, rows // 256))
     fans = min(n, 2 * groups)
+    projection, gate_weight, _, down_weight = weights
     width, ffn_local = gate_weight.shape[1], gate_weight.shape[2]
     ffn = down_weight.shape[1]
     dma = pltpu.SemaphoreType.DMA
+    bf16, f32 = jnp.bfloat16, jnp.float32
     flops = 2 * rows * width * ffn_local * 2 + 2 * rows * ffn * cols
     return pl.pallas_call(
         functools.partial(expert_kernel, n, tp),
-        out_shape=jax.ShapeDtypeStruct(outgoing.shape, jnp.bfloat16),
-        in_specs=[pl.BlockSpec(memory_space=pltpu.VMEM)]
-        + [pl.BlockSpec(memory_space=pl.ANY)] * 3,
+        out_shape=jax.ShapeDtypeStruct((row_count, cols), bf16),
+        in_specs=[pl.BlockSpec(memory_space=pltpu.VMEM)] * len(blocks)
+        + [pl.BlockSpec(memory_space=pl.ANY)] * len(weights),
         out_specs=pl.BlockSpec(memory_space=pltpu.VMEM),
         scratch_shapes=[
-            pltpu.VMEM((n, cap, width), jnp.bfloat16),
-            pltpu.VMEM((groups, rows // groups, ffn), jnp.bfloat16),
-            pltpu.VMEM((n, cap, cols), jnp.bfloat16),
-            pltpu.VMEM((width, ffn_local), jnp.bfloat16),
-            pltpu.VMEM((width, ffn_local), jnp.bfloat16),
-            pltpu.VMEM((ffn, cols), jnp.bfloat16),
-            dma((3,)),
+            pltpu.VMEM((n, cap, cols), bf16),
+            pltpu.VMEM((n, cap, cols), bf16),
+            pltpu.VMEM((row_count, wide * tp), bf16),
+            pltpu.VMEM(projection.shape, bf16),
+            pltpu.VMEM((row_count, cols), f32),
+            pltpu.VMEM((row_count, cols), bf16),
+            pltpu.VMEM((row_count, cols), bf16),
+            pltpu.VMEM((tp, 8, row_count), f32),
+            pltpu.VMEM((row_count, 128), f32),
+            pltpu.VMEM((128, row_count), f32),
+            pltpu.VMEM((row_count, 128), f32),
+            pltpu.VMEM((16, wide), bf16),
+            pltpu.VMEM((16, wide), bf16),
+            pltpu.VMEM((8, 128), f32),
+            pltpu.VMEM((n, cap, width), bf16),
+            pltpu.VMEM((groups, rows // groups, ffn), bf16),
+            pltpu.VMEM((n, cap, cols), bf16),
+            pltpu.VMEM((width, ffn_local), bf16),
+            pltpu.VMEM((width, ffn_local), bf16),
+            pltpu.VMEM((ffn, cols), bf16),
+            dma((4,)),
             dma((2,)),
             dma((n,)),
             dma((n,)),
@@ -289,21 +530,23 @@
             dma((chips, groups)),
             dma((n,)),
             dma((n,)),
+            dma((3,)),
+            dma((3,)),
+            dma((chips,)),
+            dma((chips,)),
+            dma((chips,)),
+            dma((chips,)),
+            dma((tp,)),
+            dma((tp,)),
         ],
         compiler_params=pltpu.CompilerParams(
-            collective_id=0, has_side_effects=True, vmem_limit_bytes=48 * 1024 * 1024
+            collective_id=0, has_side_effects=True, vmem_limit_bytes=56 * 1024 * 1024
         ),
         cost_estimate=pl.CostEstimate(
             flops=flops, bytes_accessed=3 * width * ffn_local * 2, transcendentals=0
         ),
-        name="experts",
-    )(outgoing, gate_weight, up_weight, down_weight)
-
-
-def passed_along(value, axis, steps):
-    count = lax.axis_size(axis)
-    initial, last = (max(0, -steps), min(count, count - steps))
-    return lax.ppermute(value, axis, [(source, source + steps) for source in range(initial, last)])
+        name="layer",
+    )(*blocks, *weights)
 
 
 def per_device(
@@ -323,62 +566,24 @@
     down_weight,
 ):
     row_count = conv_input.shape[0]
-    products = inner_gate.astype(jnp.float32) * conv_input.astype(jnp.float32)
-    own_docs = doc_ids.astype(jnp.float32)
-    tail_rows, tail_docs = passed_along((products[-2:], own_docs[-2:]), "sp", 1)
-    ext_products = jnp.concatenate([tail_rows, products], axis=0)
-    ext_docs = jnp.concatenate([tail_docs, own_docs], axis=0)
-    taps = conv_weight.astype(jnp.float32)
-    conv = taps[2] * products
-    for shift_by in (1, 2):
-        first = 2 - shift_by
-        same_doc = (ext_docs[first : first + row_count] == own_docs)[:, None]
-        conv = conv + jnp.where(
-            same_doc, taps[2 - shift_by] * ext_products[first : first + row_count], 0.0
-        )
-    branch = (outer_gate.astype(jnp.float32) * conv).astype(jnp.bfloat16)
-    cols_local = output_weight.shape[1]
-    branch_sum = jnp.dot(
-        lax.all_gather(branch, "tp", axis=1, tiled=True),
-        output_weight,
-        preferred_element_type=jnp.float32,
-    )
-    resid = (residual.astype(jnp.float32) + branch_sum).astype(jnp.bfloat16)
-    resid_wide = resid.astype(jnp.float32)
-    total_sq = lax.psum(jnp.sum(resid_wide * resid_wide, axis=1), "tp")
-    width = cols_local * lax.axis_size("tp")
-    scale = lax.rsqrt(total_sq / width + EPS)[:, None]
-    normed = (resid_wide * scale * norm_gain.astype(jnp.float32)).astype(jnp.bfloat16)
-    experts = lax.axis_size("sp")
-    capacity = 4 * row_count // experts
-    flat_experts = expert_ids.reshape(-1)
-    onehot = (flat_experts[:, None] == jnp.arange(experts, dtype=jnp.int32)[None, :]).astype(
-        jnp.int32
-    )
-    slot_rank = jnp.sum((jnp.cumsum(onehot, axis=0) - onehot) * onehot, axis=1)
-    slot_index = flat_experts * capacity + slot_rank
-    slots = slot_index.reshape(row_count, 2)
-    arrived_rows = experts * capacity
-    slot_iota = jnp.arange(arrived_rows, dtype=jnp.int32)[:, None]
-    select = (
-        (slot_iota == slots[:, 0][None, :]) | (slot_iota == slots[:, 1][None, :])
-    ).astype(jnp.bfloat16)
-    outgoing = (
-        jnp.dot(select, normed, preferred_element_type=jnp.float32)
-        .astype(jnp.bfloat16)
-        .reshape(experts, capacity, cols_local)
-    )
-    returned = expert_layer(outgoing, gate_weight, up_weight, down_weight)
-    picked = (
-        returned.reshape(arrived_rows, cols_local)[slot_index]
-        .reshape(row_count, 2, cols_local)
-        .astype(jnp.float32)
-    )
+    docs = jnp.broadcast_to(doc_ids.astype(jnp.float32)[:, None], (row_count, 128))
     mix_weight = (
         group_weight[:, None] * expert_weight / jnp.sum(expert_weight, axis=1, keepdims=True)
     )
-    routed_sum = jnp.sum(picked * mix_weight[:, :, None], axis=1)
-    return (resid_wide + routed_sum).astype(jnp.bfloat16)
+    return whole_layer(
+        (
+            outer_gate,
+            inner_gate,
+            conv_input,
+            conv_weight,
+            docs,
+            residual,
+            norm_gain[None, :],
+            expert_ids,
+            mix_weight,
+        ),
+        (output_weight, gate_weight, up_weight, down_weight),
+    )
 
 
 def solution(mesh):

time: 190 us -> 149 us (0.78)
  Pallas kernels: 125 us -> 141 us
  between operations: 13.5 us -> 0.02 us
  waiting for transfers between devices: 13.1 us -> 0 us
  other arithmetic: 12.6 us -> 2.14 us
  starting transfers between devices: 8.32 us -> 0 us
  blocking collectives: 6.06 us -> 0 us
  matrix products: 4.82 us -> 0 us
    pallas_call x1, Pallas kernels: 125 us -> 141 us  [whole_layer(): pl.pallas_call(functools.partial(expert_kernel, n, tp), out_shape=jax.Sha...]
    all_gather x1 -> x0, waiting for transfers between devices: 13.1 us -> none  [per_device(): lax.all_gather(branch, 'tp', axis=1, tiled=True)]
    ppermute x2 -> x0, starting transfers between devices: 8.32 us -> none  [passed_along(): lax.ppermute(value, axis, [(source, source + steps) for source in range(i...]
    psum x1 -> x0, blocking collectives: 6.06 us -> none  [per_device(): total_sq = lax.psum(jnp.sum(resid_wide * resid_wide, axis=1), 'tp')]
    dot_general x2 -> x0, matrix products: 4.82 us -> none  [the longest x1 3.97 us: per_device(): jnp.dot(lax.all_gather(branch, 'tp', axis=1, tiled=True), output_weight,...]
    convert_element_type x5 -> x1, other arithmetic: 5.29 us -> 0.68 us  [per_device(): doc_ids.astype(jnp.float32)[:, None]]
    reduce_sum x2 -> x0, other arithmetic: 2.74 us -> none  [the longest x1 2.64 us: per_device(): routed_sum = jnp.sum(picked * mix_weight[:, :, None], axis=1)]
    unnamed x3 -> x2, local copies, waits for them, and re-layouts: 0.82 us -> 3.34 us
  transfers between devices with their start and end apart: 3 -> 0, of which waited for: 1 -> 0; matrix products, arithmetic and copies ran while one was open for 4% -> 0% of each run, Pallas kernels for 0% -> 0%
where the time goes in v2:
time: 149 us
  Pallas kernels  141 us (95%)
  local copies, waits for them, and re-layouts  5.5 us (4%)
  other arithmetic  2.14 us (1%)
    pallas_call x1, Pallas kernels, whole_layer(): pl.pallas_call(functools.partial(expert_kernel, n, tp), out_shape=jax.Sha...  141 us
    unnamed x2, local copies, waits for them, and re-layouts  3.34 us

profile of v2, /device:TPU:0, one launch (start us, length us, event | category | flops | bytes accessed | tf_op | source)
XLA Modules:
  0.0 149.1 jit_solution(9243183420880017626)
XLA Ops:
  0.0 0.7 convert_element_type.3
  0.7 0.7 fusion
  1.4 1.3 broadcast_in_dim.5.gain_ref
  2.7 0.8 broadcast_in_dim.4.docs_ref
  3.4 0.1 copy.18
  3.6 0.8 broadcast_divide_fusion.mix_ref
  4.3 1.5 copy.20.ids_ref
  5.8 141.4 %layer.1 = bf16[256,1024]{1,0:T(8,128)(2,1)} custom-call(bf16[256,512]{1,0:T(8,128)(2,1)} %outer_ref.1, bf16[256,512]{1,0:T(8,128)(2,1)} %inner_ref.1, bf16[256,512]{1,0:T(8,128)(2,1)} %conv_ref.1, bf16[3,512]{1,0:T(4,128)(2,1)} %taps_ref.1, f32[256,128]{1,0:T(8,128)} %broadcast_in_dim.4.docs_ref, bf16[256,1024]{1,0:T(8,128)(2,1)} %residual_ref.1, ...), custom_call_target="tpu_custom_call" | custom-call | flops 12884901888 | bytes 12582912 | tf_op jit(solution)/shard_map/layer/pallas_call | solution.py:492
  147.2 1.9 %copy.22 = bf16[256,1024]{1,0:T(8,128)(2,1)} copy(bf16[256,1024]{1,0:T(8,128)(2,1)} %layer.1) | data formatting | bytes 1048576

commit v3 on v2

--- a/solution.py
+++ b/solution.py
@@ -84,6 +84,8 @@
 ):
     me = lax.axis_index("sp")
     t = lax.axis_index("tp")
+    later = [k for k in range(1, n) if k != 2]
+    order = [0, 2] + sorted(later, key=lambda k: -min(k, n - k))
     chips = tp // 2
     y, core = lax.div(t, 2), lax.rem(t, 2)
     partner = t + 1 - 2 * core
@@ -286,7 +288,7 @@
         ).astype(jnp.bfloat16)
 
     for k in range(1, n):
-        there = lax.rem(me + k, n)
+        there = lax.rem(me + order[k], n)
         choose(there)
         copy = remote(
             out_ref.at[there],
@@ -409,7 +411,7 @@
                     ret_ref.at[me],
                     r_send.at[k],
                     r_recv.at[k],
-                    (lax.rem(me + n - k, n), t),
+                    (lax.rem(me + n - order[k], n), t),
                 )
             copy.start()
             returns.append(copy)
@@ -441,14 +443,14 @@
             if k == 0:
                 returns[0].wait()
             else:
-                there = lax.rem(me + k, n)
+                there = lax.rem(me + order[k], n)
                 returns[k].wait_send()
                 remote(
                     eo.at[k], ret_ref.at[there], r_send.at[k], r_recv.at[k], (there, t)
                 ).wait_recv()
         chosen = []
         for k in members:
-            there = lax.rem(me + k, n)
+            there = lax.rem(me + order[k], n)
             here = lanes == there
             key = jnp.sum(jnp.where(here, key_col[...], 0.0), axis=1, keepdims=True)
             weight = jnp.sum(jnp.where(here, mix_col[...], 0.0), axis=1, keepdims=True)

time: 149 us -> 152 us (1.020)
  Pallas kernels: 141 us -> 144 us
    pallas_call x1, Pallas kernels: 141 us -> 144 us  [whole_layer(): pl.pallas_call(functools.partial(expert_kernel, n, tp), out_shape=jax.Sha...]
where the time goes in v3:
time: 152 us
  Pallas kernels  144 us (95%)
  local copies, waits for them, and re-layouts  5.5 us (4%)
  other arithmetic  2.14 us (1%)
    pallas_call x1, Pallas kernels, whole_layer(): pl.pallas_call(functools.partial(expert_kernel, n, tp), out_shape=jax.Sha...  144 us
    unnamed x2, local copies, waits for them, and re-layouts  3.34 us

profile of v3, /device:TPU:0, one launch (start us, length us, event | category | flops | bytes accessed | tf_op | source)
XLA Modules:
  0.0 151.9 jit_solution(643597561866447870)
XLA Ops:
  0.0 0.7 convert_element_type.3
  0.7 0.7 fusion
  1.4 1.3 broadcast_in_dim.5.gain_ref
  2.7 0.8 broadcast_in_dim.4.docs_ref
  3.4 0.1 copy.18
  3.6 0.8 broadcast_divide_fusion.mix_ref
  4.3 1.5 copy.20.ids_ref
  5.8 144.2 %layer.1 = bf16[256,1024]{1,0:T(8,128)(2,1)} custom-call(bf16[256,512]{1,0:T(8,128)(2,1)} %outer_ref.1, bf16[256,512]{1,0:T(8,128)(2,1)} %inner_ref.1, bf16[256,512]{1,0:T(8,128)(2,1)} %conv_ref.1, bf16[3,512]{1,0:T(4,128)(2,1)} %taps_ref.1, f32[256,128]{1,0:T(8,128)} %broadcast_in_dim.4.docs_ref, bf16[256,1024]{1,0:T(8,128)(2,1)} %residual_ref.1, ...), custom_call_target="tpu_custom_call" | custom-call | flops 12884901888 | bytes 12582912 | tf_op jit(solution)/shard_map/layer/pallas_call | solution.py:494
  150.0 1.9 %copy.22 = bf16[256,1024]{1,0:T(8,128)(2,1)} copy(bf16[256,1024]{1,0:T(8,128)(2,1)} %layer.1) | data formatting | bytes 1048576
